TPU v7x, 128 devices: a whole 4x4x4 slice. The times are simulated.
128 devices in a mesh: sp: 32 (over z, y, core), tp: 4 (over x).
Axes of the slice: x: 4, y: 4, z: 4, core: 2. Of those that a mesh axis runs over, the one named last changes fastest.
Arguments:
- tokens: bfloat16 [32768, 2048], P('sp', 'tp'), may hold values from -6 to 6
- input_norm_gain: float32 [2048], replicated, may hold values from 0.1 to 1.9
- pooling_input_matrix: bfloat16 [2048, 512], P(None, 'tp'), may hold values from -0.125 to 0.125
- query_projection_matrix: bfloat16 [2048, 1024], P(None, 'tp'), may hold values from -0.125 to 0.125
- key_projection_matrix: bfloat16 [2048, 1024], P(None, 'tp'), may hold values from -0.125 to 0.125
- value_projection_matrix: bfloat16 [2048, 1024], P(None, 'tp'), may hold values from -0.125 to 0.125
- output_gate_matrix: bfloat16 [2048, 1024], P(None, 'tp'), may hold values from -0.125 to 0.125
- input_gate_matrix: bfloat16 [2048, 2, 8], replicated
- forget_gate_matrix: bfloat16 [2048, 2, 8], replicated, may hold values from -0.125 to 0.125
- forget_gate_bias: float32 [2, 8], replicated
- log_forget_scale: float32 [2, 32768], P(None, 'sp'), may hold values from 0.35 to 2.8
- extra_log_forget: float32 [2, 32768], P(None, 'sp'), may hold values from -0.7 to 0, as said below
- starting_memory: float32 [2, 8, 128, 128], P(None, 'tp'), may hold values from -3 to 3
- starting_normalizer: float32 [2, 8, 128], P(None, 'tp'), may hold values from -3 to 3
- starting_log_scale: float32 [2, 8], P(None, 'tp'), may hold values from 2 to 5
- pooling_group_map: bfloat16 [4, 128, 128], replicated, may hold values from -0.5 to 0.5
- pooling_channel_scale: float32 [512], replicated, may hold values from 0.1 to 1.9
- memory_head_gain: float32 [1024], replicated, may hold values from 0.1 to 1.9
- pooling_output_matrix: bfloat16 [512, 2048], replicated, may hold values from -0.25 to 0.25
- memory_output_matrix: bfloat16 [1024, 2048], replicated, may hold values from -0.1875 to 0.1875
Outputs:
- mixed_out: bfloat16 [32768, 2048], P(('sp', 'tp'))
Inputs may be any that keep to these rules, and one draw needn't show every extreme that they name: `extra_log_forget`: at most three nonzero entries in each direction.
All inputs are finite; a program needn't handle non-finite values.
Results may differ from a plain program's by a relative error of at most 0.0091.
Values may be sent and summed in bfloat16 or wider, within the bound.
A program may use at most 128 MiB of HBM per device.

v0:
```python
import jax
import jax.numpy as jnp
from jax import lax
from jax.sharding import PartitionSpec as P

DH = 128
BLOCK = 128
NEG_BIG = -1e30
LN_EPS = 1e-05
HEAD_EPS = 1e-06
RIM_ROWS = 8


def extended(block, sides, width):
    for axis, dim in sides:
        count = lax.axis_size(axis)
        forward = [(i, i + 1) for i in range(count - 1)]
        backward = [(target, source) for source, target in forward]
        low = lax.ppermute(
            lax.slice_in_dim(block, block.shape[dim] - width, None, axis=dim), axis, forward
        )
        high = lax.ppermute(lax.slice_in_dim(block, 0, width, axis=dim), axis, backward)
        block = jnp.concatenate([low, block, high], axis=dim)
    return block


def block_step(carried, pieces):
    memory, normer, maxlog = carried
    q_blk, k_blk, v_blk, i_blk, f_blk = pieces
    lower_mask = jnp.tril(jnp.ones((BLOCK, BLOCK), dtype=bool))
    cumulative = jnp.cumsum(f_blk, axis=-1)
    exponent = jnp.where(
        lower_mask, cumulative[:, :, None] - cumulative[:, None, :] + i_blk[:, None, :], NEG_BIG
    )
    carried_log = cumulative + maxlog[:, None]
    row_max = jnp.maximum(carried_log, exponent.max(-1))
    fading = jnp.exp(carried_log - row_max)
    scores = jnp.einsum("htd,hsd->hts", q_blk, k_blk) * jnp.exp(exponent - row_max[:, :, None])
    numerator = fading[:, :, None] * jnp.einsum("hvk,htk->htv", memory, q_blk) + jnp.einsum(
        "hts,hsv->htv", scores, v_blk
    )
    denominator = fading * jnp.einsum("hk,htk->ht", normer, q_blk) + scores.sum(-1)
    summed = cumulative[:, -1]
    weight_log = summed[:, None] - cumulative + i_blk
    new_max = jnp.maximum(summed + maxlog, weight_log.max(-1))
    carry_scale = jnp.exp(summed + maxlog - new_max)
    weights = jnp.exp(weight_log - new_max[:, None])
    memory = carry_scale[:, None, None] * memory + jnp.einsum(
        "hsv,hsk->hvk", v_blk * weights[:, :, None], k_blk
    )
    normer = carry_scale[:, None] * normer + jnp.einsum("hs,hsk->hk", weights, k_blk)
    return ((memory, normer, new_max), (numerator, denominator, row_max))


def to_blocks(source):
    return jnp.moveaxis(
        source.reshape((source.shape[0], source.shape[1] // BLOCK, BLOCK) + source.shape[2:]), 1, 0
    )


def from_blocks(source):
    return jnp.moveaxis(source, 0, 1).reshape(
        (source.shape[1], source.shape[0] * source.shape[2]) + source.shape[3:]
    )


def local_pass(query_heads, key_heads, value_heads, log_in, log_forget_gate):
    head_count = query_heads.shape[0]
    head_size = query_heads.shape[2]
    initial = (
        jnp.zeros((head_count, head_size, head_size), jnp.float32),
        jnp.zeros((head_count, head_size), jnp.float32),
        jnp.full((head_count,), NEG_BIG, jnp.float32),
    )
    finals, outputs = lax.scan(
        block_step,
        initial,
        tuple(
            (
                to_blocks(member)
                for member in (query_heads, key_heads, value_heads, log_in, log_forget_gate)
            )
        ),
    )
    numerator, denominator, row_max = (from_blocks(member) for member in outputs)
    falls = jnp.cumsum(log_forget_gate, axis=1)
    return ((falls[:, -1],) + finals, (numerator, denominator, row_max, falls))


def join_states(earlier, later):
    early_fall, early_memory, early_normer, early_max = earlier
    late_fall, late_memory, late_normer, late_max = later
    merged_max = jnp.maximum(early_max + late_fall, late_max)
    early_weight = jnp.exp(early_max + late_fall - merged_max)
    late_weight = jnp.exp(late_max - merged_max)
    return (
        late_fall,
        early_weight[..., None, None] * early_memory + late_weight[..., None, None] * late_memory,
        early_weight[..., None] * early_normer + late_weight[..., None] * late_normer,
        merged_max,
    )


def prefix_from_all(gathered, position, from_later):
    falls, memories, normers, maxima = gathered
    order = jnp.arange(falls.shape[0], dtype=jnp.int32)
    inclusive = jnp.cumsum(falls, axis=0)
    exclusive = inclusive - falls
    if from_later:
        valid = order > position
        between = exclusive - inclusive[position][None]
        total_fall = inclusive[-1] - inclusive[position]
    else:
        valid = order < position
        between = exclusive[position][None] - inclusive
        total_fall = exclusive[position]
    log_weight = jnp.where(valid[:, None], maxima + between, NEG_BIG)
    joint_max = jnp.max(log_weight, axis=0)
    weights = jnp.where(valid[:, None], jnp.exp(log_weight - joint_max[None]), 0.0)
    memory = jnp.einsum("jh,jhvk->hvk", weights, memories)
    normer = jnp.einsum("jh,jhk->hk", weights, normers)
    return (total_fall, memory, normer, joint_max)


def finish(local_terms, entering, query_heads):
    numerator, denominator, row_max, falls = local_terms
    fall_in, memory, normer, max_in = entering
    state_log = falls + max_in[:, None]
    joint_max = jnp.maximum(row_max, state_log)
    local_weight = jnp.exp(row_max - joint_max)
    state_weight = jnp.exp(state_log - joint_max)
    full_numerator = local_weight[..., None] * numerator + state_weight[..., None] * jnp.einsum(
        "hvk,htk->htv", memory, query_heads
    )
    full_denominator = local_weight * denominator + state_weight * jnp.einsum(
        "hk,htk->ht", normer, query_heads
    )
    return full_numerator / jnp.maximum(jnp.abs(full_denominator), 1.0)[..., None]


def per_device(
    tokens,
    input_norm_gain,
    pooling_input_matrix,
    query_projection_matrix,
    key_projection_matrix,
    value_projection_matrix,
    output_gate_matrix,
    input_gate_matrix,
    forget_gate_matrix,
    forget_gate_bias,
    log_forget_scale,
    extra_log_forget,
    starting_memory,
    starting_normalizer,
    starting_log_scale,
    pooling_group_map,
    pooling_channel_scale,
    memory_head_gain,
    pooling_output_matrix,
    memory_output_matrix,
):
    local_rows = tokens.shape[0]
    own_width = tokens.shape[1]
    model_width = own_width * lax.axis_size("tp")
    group_index = lax.axis_index("tp")
    seq_index = lax.axis_index("sp")
    group_dim = pooling_input_matrix.shape[1]
    head_local = query_projection_matrix.shape[1] // DH
    mem_width = head_local * DH
    main_weight = jnp.concatenate(
        [
            pooling_input_matrix,
            query_projection_matrix,
            key_projection_matrix,
            value_projection_matrix,
            output_gate_matrix,
        ],
        axis=1,
    )
    gate_in = lax.dynamic_slice_in_dim(input_gate_matrix, group_index * head_local, head_local, 2)
    gate_fg = lax.dynamic_slice_in_dim(forget_gate_matrix, group_index * head_local, head_local, 2)
    gate_weight = jnp.concatenate([gate_in, gate_fg], axis=1).reshape(model_width, 4 * head_local)
    whole_rows = lax.all_gather(tokens, "tp", axis=1, tiled=True)
    floats = whole_rows.astype(jnp.float32)
    mean_row = jnp.sum(floats, axis=1) / model_width
    variance = jnp.sum(floats * floats, axis=1) / model_width - mean_row * mean_row
    normed = (
        (floats - mean_row[:, None]) * lax.rsqrt(variance + LN_EPS)[:, None] * input_norm_gain
    ).astype(jnp.bfloat16)
    projected = jnp.dot(normed, main_weight, preferred_element_type=jnp.float32)
    gate_pre = jnp.dot(normed, gate_weight, preferred_element_type=jnp.float32)
    pool_in = projected[:, :group_dim].astype(jnp.bfloat16)
    queries = projected[:, group_dim : group_dim + mem_width].astype(jnp.bfloat16)
    key_rows = projected[:, group_dim + mem_width : group_dim + 2 * mem_width].astype(jnp.bfloat16)
    value_rows = projected[:, group_dim + 2 * mem_width : group_dim + 3 * mem_width].astype(
        jnp.bfloat16
    )
    out_gate = projected[:, group_dim + 3 * mem_width :].astype(jnp.bfloat16)
    gate_pre = gate_pre.reshape(local_rows, 2, 2, head_local)
    log_in = gate_pre[:, 0]
    bias_own = lax.dynamic_slice_in_dim(forget_gate_bias, group_index * head_local, head_local, 1)
    log_forget_gate = (
        jax.nn.log_sigmoid(gate_pre[:, 1] + bias_own[None]) * log_forget_scale.T[:, :, None]
        + extra_log_forget.T[:, :, None]
    )

    def heads_of(source, factor):
        return (
            (source.astype(jnp.float32) * factor)
            .reshape(local_rows, head_local, DH)
            .transpose(1, 0, 2)
        )

    query_heads = heads_of(queries, 1.0)
    key_heads = heads_of(key_rows, DH ** (-0.5))
    value_heads = heads_of(value_rows, 1.0)
    forward_summary, forward_local = local_pass(
        query_heads, key_heads, value_heads, log_in[:, 0].T, log_forget_gate[:, 0].T
    )
    flipped_query = query_heads[:, ::-1]
    backward_summary, backward_local = local_pass(
        flipped_query,
        key_heads[:, ::-1],
        value_heads[:, ::-1],
        log_in[:, 1].T[:, ::-1],
        log_forget_gate[:, 1].T[:, ::-1],
    )
    rimmed = extended(pool_in, (("sp", 0),), RIM_ROWS).astype(jnp.float32)
    half_span = jnp.left_shift(jnp.int32(1), group_index)
    grouped = pool_in.astype(jnp.float32)
    pooled = jnp.zeros_like(grouped)
    for offset in range(-RIM_ROWS, RIM_ROWS):
        inside = ((offset >= -half_span) & (offset < half_span)).astype(jnp.float32)
        pooled = pooled + inside * rimmed[RIM_ROWS + offset : RIM_ROWS + offset + local_rows]
    positions = seq_index * local_rows + jnp.arange(local_rows, dtype=jnp.int32)
    total_rows = local_rows * lax.axis_size("sp")
    counts = (
        jnp.minimum(positions + half_span, total_rows) - jnp.maximum(positions - half_span, 0)
    ).astype(jnp.float32)
    contrast = (pooled / counts[:, None] - grouped).astype(jnp.bfloat16)
    map_own = lax.dynamic_index_in_dim(pooling_group_map, group_index, 0, keepdims=False)
    scale_own = lax.dynamic_slice_in_dim(
        pooling_channel_scale, group_index * group_dim, group_dim, 0
    )
    pool_out = (jnp.dot(contrast, map_own, preferred_element_type=jnp.float32) * scale_own).astype(
        jnp.bfloat16
    )
    stacked = tuple(
        (
            jnp.stack([forward_part, backward_part])[None]
            for forward_part, backward_part in zip(forward_summary, backward_summary)
        )
    )
    gathered = lax.all_gather(stacked, "sp", axis=0, tiled=True)
    forward_prefix = prefix_from_all(tuple((member[:, 0] for member in gathered)), seq_index, False)
    backward_prefix = prefix_from_all(tuple((member[:, 1] for member in gathered)), seq_index, True)

    def initial_state(direction):
        return (
            jnp.zeros((head_local,), jnp.float32),
            starting_memory[direction],
            starting_normalizer[direction],
            starting_log_scale[direction],
        )

    forward = finish(forward_local, join_states(initial_state(0), forward_prefix), query_heads)
    backward = finish(backward_local, join_states(initial_state(1), backward_prefix), flipped_query)
    hidden = forward + backward[:, ::-1]
    head_mean = jnp.mean(hidden, axis=-1, keepdims=True)
    head_var = jnp.mean(jnp.square(hidden - head_mean), axis=-1, keepdims=True)
    gain_heads = lax.dynamic_slice_in_dim(
        memory_head_gain, group_index * mem_width, mem_width, 0
    ).reshape(head_local, DH)
    scaled = (hidden - head_mean) * lax.rsqrt(head_var + HEAD_EPS) * gain_heads[:, None, :]
    mem_out = (
        scaled.transpose(1, 0, 2).reshape(local_rows, mem_width)
        * jax.nn.sigmoid(out_gate.astype(jnp.float32))
    ).astype(jnp.bfloat16)
    mixed = jnp.concatenate([pool_out, mem_out], axis=1)
    owned = lax.all_to_all(mixed, "tp", split_axis=0, concat_axis=1, tiled=True)
    owner_rows = owned.shape[0]
    owned = owned.reshape(owner_rows, lax.axis_size("tp"), group_dim + mem_width)
    pool_part = owned[:, :, :group_dim].reshape(owner_rows, lax.axis_size("tp") * group_dim)
    mem_part = owned[:, :, group_dim:].reshape(owner_rows, lax.axis_size("tp") * mem_width)
    result = jnp.dot(
        pool_part, pooling_output_matrix, preferred_element_type=jnp.float32
    ) + jnp.dot(mem_part, memory_output_matrix, preferred_element_type=jnp.float32)
    return result.astype(jnp.bfloat16)


def solution(mesh):
    placed = (
        P("sp", "tp"),
        P(),
        P(None, "tp"),
        P(None, "tp"),
        P(None, "tp"),
        P(None, "tp"),
        P(None, "tp"),
        P(),
        P(),
        P(),
        P(None, "sp"),
        P(None, "sp"),
        P(None, "tp", None, None),
        P(None, "tp", None),
        P(None, "tp"),
        P(),
        P(),
        P(),
        P(),
        P(),
    )
    return jax.shard_map(
        per_device, mesh=mesh, in_specs=placed, out_specs=P(("sp", "tp"), None), check_vma=False
    )
```

profile of v0, /device:TPU:1, one launch (start us, length us, event | category | flops | bytes accessed | tf_op | source)
XLA Modules:
  0.0 383.7 jit_solution(3305362146877481871)
XLA Ops:
  9.4 1.9 constant_dynamic-update-slice_fusion.8
  11.3 2.3 constant_dynamic-update-slice_fusion.7
  16.9 43.3 %all-gather.9.cloned.1.call-done = bf16[1024,2048]{1,0:T(8,128)(2,1)} async-done(((bf16[1024,512]{1,0:T(8,128)(2,1)}), bf16[1024,2048]{1,0:T(8,128)(2,1)}) %all-gather.9.cloned.1.call-update) | async-done | bytes 4194320 | tf_op jit(solution)/shard_map/all_gather | solution.py:184
  60.2 3.6 convert_reduce_fusion
  63.9 8.5 %convolution_convert_fusion = bf16[1024,1152]{1,0:T(8,128)(2,1)S(1)} fusion(bf16[2048,1152]{1,0:T(8,128)(2,1)} %constant_dynamic-update-slice_fusion.4, bf16[1024,2048]{1,0:T(8,128)(2,1)S(1)} %copy-done.5, f32[2048]{0:T(1024)S(1)} %copy-done.21, f32[1024]{0:T(1024)S(1)} %get-tuple-element.398, f32[1024]{0:T(1024)S(1)} %get-tuple-element.397), kind=kOutput, calls=%fused_computation.125 | convolution fusion | flops 4843503616 | bytes 11288576 | tf_op jit(solution)/shard_map/dot_general | solution.py:191
  72.4 1.5 multiply_bitcast_fusion
  74.7 1.3 copy_bitcast_fusion
  75.9 5.1 %rev.22 = bf16[2,1024,128]{2,1,0:T(8,128)(2,1)} reverse(bf16[2,1024,128]{2,1,0:T(8,128)(2,1)S(1)} %get-tuple-element.407), dimensions={1} | reverse | bytes 1048576 | tf_op jit(solution)/shard_map/rev | solution.py:221
  81.0 3.7 fusion.70
  86.3 1.3 copy.211
  87.6 5.1 %rev.20 = f32[2,1024,128]{2,1,0:T(8,128)} reverse(f32[2,1024,128]{2,1,0:T(8,128)S(1)} %bitcast.498), dimensions={1} | reverse | bytes 2097152 | tf_op jit(solution)/shard_map/rev | solution.py:225
  92.7 8.2 %rev.21 = bf16[2,1024,128]{2,1,0:T(8,128)(2,1)} reverse(bf16[2,1024,128]{2,1,0:T(8,128)(2,1)} %get-tuple-element.381), dimensions={1} | reverse | bytes 1048576 | tf_op jit(solution)/shard_map/rev | solution.py:224
  101.0 1.9 copy.212
  104.0 66.0 %while.43 = (s32[]{:T(128)}, f32[2,128,128]{2,1,0:T(8,128)S(1)}, f32[2,128]{1,0:T(2,128)S(1)}, f32[2]{0:T(128)S(1)}, f32[8,2,128,128]{3,2,1,0:T(8,128)}, /*index...) while((s32[]{:T(128)}, f32[2,128,128]{2,1,0:T(8,128)S(1)}, ...), condition=%wide.region_18.19_spmd.clone, body=%wide.region_13.18_spmd.clone.sunk | while | flops 34327816 | bytes 1600317 | solution.py:75
  110.4 1.8 fusion.266
  118.7 1.8 fusion.266
  126.9 1.8 fusion.266
  135.1 1.8 fusion.266
  143.4 1.8 fusion.266
  151.6 1.8 fusion.266
  159.9 1.8 fusion.266
  168.1 1.8 fusion.266
  169.9 1.9 copy.213
  172.9 58.1 %while.42 = (s32[]{:T(128)}, f32[2,128,128]{2,1,0:T(8,128)S(1)}, f32[2,128]{1,0:T(2,128)S(1)}, f32[2]{0:T(128)S(1)}, f32[8,2,128,128]{3,2,1,0:T(8,128)}, /*index...) while((s32[]{:T(128)}, f32[2,128,128]{2,1,0:T(8,128)S(1)}, ...), condition=%wide.region_7.8_spmd.clone, body=%wide.region_2.7_spmd.clone.sunk | while | flops 34327816 | bytes 1600821 | solution.py:75
  231.8 1.3 dynamic_slice.60
  236.3 25.2 %all-gather.4 = f32[32,2,2]{2,1,0:T(2,128)S(1)} all-gather(f32[1,2,2]{2,1,0:T(2,128)S(1)} %maximum_bitcast_fusion), channel_id=2, replica_groups=mesh['sp'=32,'tp'=4] {'sp'}, dimensions={0}, use_global_device_ids=true | all-gather | bytes 528 | tf_op jit(solution)/shard_map/all_gather | solution.py:255
  261.7 23.6 %all-gather.5 = f32[32,2,2]{2,1,0:T(2,128)S(1)} all-gather(f32[1,2,2]{2,1,0:T(2,128)S(1)} %maximum_bitcast_fusion.1), channel_id=3, replica_groups=mesh['sp'=32,'tp'=4] {'sp'}, dimensions={0}, use_global_device_ids=true | all-gather | bytes 528 | tf_op jit(solution)/shard_map/all_gather | solution.py:255
  286.8 2.1 collective-permute-start.1
  288.9 3.5 collective-permute-start
  292.4 22.6 %all-gather.3 = bf16[64,2,128]{2,1,0:T(2,128)(2,1)S(1)} all-gather(bf16[2,2,128]{2,1,0:T(2,128)(2,1)S(1)} %pad_maximum_fusion.3), channel_id=5, replica_groups=mesh['sp'=32,'tp'=4] {'sp'}, dimensions={0}, use_global_device_ids=true | all-gather | bytes 33792 | tf_op jit(solution)/shard_map/all_gather | solution.py:255
  315.6 1.3 fusion.177
  317.0 1.3 fusion.83
  318.4 2.6 copy.115
  321.0 2.4 reshape.649
  323.6 1.3 copy.109
  324.9 2.4 reshape.646
  327.4 2.1 fusion.82
  329.5 4.2 %slice_bitcast_fusion.1 = (bf16[32,2,128,128]{3,2,1,0:T(8,128)(2,1)}, bf16[32,2,128,128]{3,2,1,0:T(8,128)(2,1)S(1)}) fusion(bf16[32,2,2,128,128]{4,3,2,1,0:T(8,128)(2,1)} %bitcast.502), kind=kLoop, calls=%fused_computation.118 | loop fusion | bytes 8388608 | tf_op jit(solution)/shard_map/squeeze | solution.py:256
  333.7 1.2 fusion.72
  335.0 1.3 fusion.81
  336.4 9.4 %rev.23 = f32[2,1024,128]{1,2,0:T(8,128)} reverse(f32[2,1024,128]{1,2,0:T(8,128)} %fusion.81), dimensions={1} | reverse | bytes 2097152 | tf_op jit(solution)/shard_map/rev | solution.py:269
  345.7 2.8 fusion.74
  348.6 2.0 fusion.176
  351.9 1.6 copy.152
  353.4 1.3 multiply_convert_fusion
  356.0 15.5 %all_to_all.16 = bf16[4,256,384]{1,2,0:T(8,128)(2,1)S(1)} all-to-all(bf16[4,256,384]{1,2,0:T(8,128)(2,1)} %copy.118), channel_id=1, replica_groups=mesh['sp'=32,'tp'=4] {'tp'}, dimensions={0} | all-to-all | bytes 1572864 | tf_op jit(solution)/shard_map/all_to_all | solution.py:281
  371.6 3.5 fusion.178
  375.1 1.7 fusion.76
  (422 shorter events, 128.8 us)
Async XLA Ops:
  6.5 368.6 %copy-start = (bf16[512,2048]{1,0:T(8,128)(2,1)S(1)}, bf16[512,2048]{1,0:T(8,128)(2,1)}, u32[]{:S(2)}) copy-start(bf16[512,2048]{1,0:T(8,128)(2,1)} %param.42) | copy-start | bytes 6291460
  6.5 7.1 %copy-start.8 = (bf16[2048,256]{1,0:T(8,128)(2,1)S(1)}, bf16[2048,256]{1,0:T(8,128)(2,1)}, u32[]{:S(2)}) copy-start(bf16[2048,256]{1,0:T(8,128)(2,1)} %param.28) | copy-start | bytes 3145732
  6.5 53.7 %all-gather.9.cloned.1.call-start = ((), (), s32[]{:S(2)}) async-start(), calls=%async_computation.1 | async-start | bytes 5242880 | tf_op jit(solution)/shard_map/all_gather | solution.py:184
  7.3 322.2 %all-gather.11.cloned.1.call-start = ((), (), s32[]{:S(2)}) async-start(), calls=%async_computation.2 | async-start | bytes 4325376 | tf_op jit(solution)/shard_map/all_gather | solution.py:255
  8.4 6.2 %copy-start.9 = (bf16[2048,256]{1,0:T(8,128)(2,1)S(1)}, bf16[2048,256]{1,0:T(8,128)(2,1)}, u32[]{:S(2)}) copy-start(bf16[2048,256]{1,0:T(8,128)(2,1)} %param.29) | copy-start | bytes 3145732
  8.5 7.3 %copy-start.10 = (bf16[2048,256]{1,0:T(8,128)(2,1)S(1)}, bf16[2048,256]{1,0:T(8,128)(2,1)}, u32[]{:S(2)}) copy-start(bf16[2048,256]{1,0:T(8,128)(2,1)} %param.30) | copy-start | bytes 3145732
  14.7 49.2 %copy-start.21 = (f32[2048]{0:T(1024)S(1)}, f32[2048]{0:T(1024)}, u32[]{:S(2)}) copy-start(f32[2048]{0:T(1024)} %param.25) | copy-start | bytes 24580
  60.2 3.6 copy-start.5
  72.4 3.5 copy-start.7
  73.9 0.8 copy-start.1
  75.9 8.8 %copy-start.3 = (bf16[2,1024,128]{2,1,0:T(8,128)(2,1)}, bf16[2,1024,128]{2,1,0:T(8,128)(2,1)S(1)}, u32[]{:S(2)}) copy-start(bf16[2,1024,128]{2,1,0:T(8,128)(2,1)S(1)} %get-tuple-element.407) | copy-start | bytes 1572868
  81.0 3.7 copy-start.12
  81.0 3.7 copy-start.13
  172.9 113.0 %copy-start.15 = (f32[2,2]{1,0:T(2,128)S(1)}, f32[2,2]{1,0:T(2,128)}, u32[]{:S(2)}) copy-start(f32[2,2]{1,0:T(2,128)} %param.38) | copy-start | bytes 52
  172.9 142.5 %copy-start.14 = (f32[2,2,128]{2,1,0:T(2,128)S(1)}, f32[2,2,128]{2,1,0:T(2,128)}, u32[]{:S(2)}) copy-start(f32[2,2,128]{2,1,0:T(2,128)} %param.37) | copy-start | bytes 6148
  231.0 92.6 %copy-start.6 = (f32[8,2,128,128]{3,2,1,0:T(8,128)S(1)}, f32[8,2,128,128]{3,2,1,0:T(8,128)}, u32[]{:S(2)}) copy-start(f32[8,2,128,128]{3,2,1,0:T(8,128)} %get-tuple-element.142) | copy-start | bytes 3145732
  286.8 40.5 %collective-permute-start.1 = (bf16[8,128]{1,0:T(8,128)(2,1)S(1)}, bf16[8,128]{1,0:T(8,128)(2,1)S(1)}, u32[]{:S(2)}, u32[]{:S(2)}) collective-permute-start(bf16[8,128]{1,0:T(8,128)(2,1)S(1)} %get-tuple-element.374), channel_id=1, source_target_pairs={{4,0},{8,4},{12,8},{16,12},{20,16},{24,20},{28,24},{32,28},{36,32}... | collective-permute-start | bytes 6152 | tf_op jit(solution)/shard_map/ppermute | solution.py:22
  288.9 38.4 %collective-permute-start = (bf16[8,128]{1,0:T(8,128)(2,1)S(1)}, bf16[8,128]{1,0:T(8,128)(2,1)S(1)}, u32[]{:S(2)}, u32[]{:S(2)}) collective-permute-start(bf16[8,128]{1,0:T(8,128)(2,1)S(1)} %get-tuple-element.373), channel_id=1, source_target_pairs={{0,4},{4,8},{8,12},{12,16},{16,20},{20,24},{24,28},{28,32},{32,36}... | collective-permute-start | bytes 6152 | tf_op jit(solution)/shard_map/ppermute | solution.py:19
  315.1 1.9 copy-start.16
  315.1 0.5 copy-start.18
  318.4 8.9 %slice-start = ((bf16[1024,1152]{1,0:T(8,128)(2,1)}), bf16[1024,128]{1,0:T(8,128)(2,1)S(1)}, s32[]{:S(2)}) async-start(bf16[1024,1152]{1,0:T(8,128)(2,1)} %copy-done.7), calls=%async_computation.3 | async-start | bytes 524288 | tf_op jit(solution)/shard_map/slice | solution.py:193
  318.4 8.9 %copy-start.22 = (f32[128]{0:T(128)S(1)}, f32[128]{0:T(128)}, u32[]{:S(2)}) copy-start(f32[128]{0:T(128)} %dynamic_slice.60) | copy-start | bytes 1540
  329.5 5.5 %copy-start.4 = (bf16[2,1024,128]{2,1,0:T(8,128)(2,1)S(1)}, bf16[2,1024,128]{2,1,0:T(8,128)(2,1)}, u32[]{:S(2)}) copy-start(bf16[2,1024,128]{2,1,0:T(8,128)(2,1)} %rev.22) | copy-start | bytes 1572868
  329.5 5.5 %copy-start.11 = (f32[2,1024,128]{1,2,0:T(8,128)S(1)}, f32[2,1024,128]{1,2,0:T(8,128)}, u32[]{:S(2)}) copy-start(f32[2,1024,128]{1,2,0:T(8,128)} %reshape.649) | copy-start | bytes 3145732
  329.5 5.5 %copy-start.19 = (f32[2]{0:T(128)S(1)}, f32[2]{0:T(128)}, u32[]{:S(2)}) copy-start(f32[2]{0:T(128)} %copy-done.18) | copy-start | bytes 28
  329.5 5.5 %copy-start.20 = (f32[2,2,128,128]{3,2,1,0:T(8,128)S(1)}, f32[2,2,128,128]{3,2,1,0:T(8,128)}, u32[]{:S(2)}) copy-start(f32[2,2,128,128]{3,2,1,0:T(8,128)} %param.36) | copy-start | bytes 786436
  335.0 13.6 %copy-start.2 = (bf16[128,2,8,128]{3,2,1,0:T(8,128)(2,1)S(1)}, bf16[128,2,8,128]{3,2,1,0:T(8,128)(2,1)}, u32[]{:S(2)}) copy-start(bf16[128,2,8,128]{3,2,1,0:T(8,128)(2,1)} %copy-done.1) | copy-start | bytes 1572868
  335.0 13.6 %copy-start.17 = (f32[2]{0:T(128)S(1)}, f32[2]{0:T(128)}, u32[]{:S(2)}) copy-start(f32[2]{0:T(128)} %copy-done.16) | copy-start | bytes 28
Sparse Core Ops, SparseCore 0:
  9.0 51.1 all-gather.8
  231.8 47.1 all-gather.10
where the time goes:
time: 390 us; the launch traced here: 384 us
  matrix products  134 us (34%)
  blocking collectives  86.9 us (22%)
  local copies, waits for them, and re-layouts  71.2 us (18%)
  waiting for transfers between devices  44.1 us (11%)
  other arithmetic  26.8 us (7%)
  between operations  14 us (4%)
  starting transfers between devices  5.59 us (1%)
    all_gather x3, blocking collectives, per_device(): gathered = lax.all_gather(stacked, 'sp', axis=0, tiled=True)  71.4 us
    all_gather x1, waiting for transfers between devices, per_device(): whole_rows = lax.all_gather(tokens, 'tp', axis=1, tiled=True)  43.3 us
    dot_general x16, matrix products, block_step(): jnp.einsum('hts,hsv->htv', scores, v_blk)  21.4 us
    dot_general x16, matrix products, block_step(): jnp.einsum('hsv,hsk->hvk', v_blk * weights[:, :, None], k_blk)  18.7 us
    dot_general x16, matrix products, block_step(): jnp.einsum('htd,hsd->hts', q_blk, k_blk)  16.9 us
    dot_general x16, matrix products, block_step(): jnp.einsum('hvk,htk->htv', memory, q_blk)  16.6 us
    dot_general x16, matrix products, block_step(): jnp.einsum('hk,htk->ht', normer, q_blk)  15.5 us
    all_to_all x1, blocking collectives, per_device(): owned = lax.all_to_all(mixed, 'tp', split_axis=0, concat_axis=1, tiled=True)  15.5 us
  transfers between devices with their start and end apart: 4, of which 1 were waited for; matrix products, arithmetic and copies ran while one was open for 8% of the time, Pallas kernels for 0%

commit v1 on v0

--- a/solution.py
+++ b/solution.py
@@ -181,7 +181,11 @@
     gate_in = lax.dynamic_slice_in_dim(input_gate_matrix, group_index * head_local, head_local, 2)
     gate_fg = lax.dynamic_slice_in_dim(forget_gate_matrix, group_index * head_local, head_local, 2)
     gate_weight = jnp.concatenate([gate_in, gate_fg], axis=1).reshape(model_width, 4 * head_local)
-    whole_rows = lax.all_gather(tokens, "tp", axis=1, tiled=True)
+    guide_the_shards = lambda vec, lane_axis, d0: jnp.concatenate(
+        lax.all_to_all(jnp.stack([vec for _ in range(lax.axis_size(lane_axis))]), lane_axis, 0, 0),
+        axis=d0,
+    )
+    whole_rows = guide_the_shards(tokens, "tp", 1)
     floats = whole_rows.astype(jnp.float32)
     mean_row = jnp.sum(floats, axis=1) / model_width
     variance = jnp.sum(floats * floats, axis=1) / model_width - mean_row * mean_row

time: 390 us -> 408 us (1.046)
  local copies, waits for them, and re-layouts: 71.2 us -> 82.5 us
  waiting for transfers between devices: 44.1 us -> 39.7 us
  blocking collectives: 86.9 us -> 91.3 us
  starting transfers between devices: 5.59 us -> 9.92 us
  other arithmetic: 26.8 us -> 31.1 us
    all_gather x1 -> x0, waiting for transfers between devices: 43.3 us -> none  [per_device(): whole_rows = lax.all_gather(tokens, 'tp', axis=1, tiled=True)]
    all_to_all x0 -> x1, waiting for transfers between devices: none -> 39.7 us  [per_device(): lax.all_to_all(jnp.stack([vec for _ in range(lax.axis_size(lane_axis))]),...]
    all_to_all x0 -> x1, local copies, waits for them, and re-layouts: none -> 6.31 us  [per_device(): lax.all_to_all(jnp.stack([vec for _ in range(lax.axis_size(lane_axis))]),...]
    all_to_all x0 -> x1, starting transfers between devices: none -> 5.02 us  [per_device(): lax.all_to_all(jnp.stack([vec for _ in range(lax.axis_size(lane_axis))]),...]
    all_gather x3, blocking collectives: 71.4 us -> 75.7 us  [per_device(): gathered = lax.all_gather(stacked, 'sp', axis=0, tiled=True)]
  transfers between devices with their start and end apart: 4 -> 4, of which waited for: 1 -> 1; matrix products, arithmetic and copies ran while one was open for 8% -> 7% of each run, Pallas kernels for 0% -> 0%
where the time goes in v1:
time: 408 us; the launch traced here: 400 us
  matrix products  132 us (32%)
  blocking collectives  91.3 us (22%)
  local copies, waits for them, and re-layouts  82.5 us (20%)
  waiting for transfers between devices  39.7 us (10%)
  other arithmetic  31.1 us (8%)
  between operations  14 us (3%)
  starting transfers between devices  9.92 us (2%)
    all_gather x3, blocking collectives, per_device(): gathered = lax.all_gather(stacked, 'sp', axis=0, tiled=True)  75.7 us
    all_to_all x1, waiting for transfers between devices, per_device(): lax.all_to_all(jnp.stack([vec for _ in range(lax.axis_size(lane_axis))]),...  39.7 us
    dot_general x16, matrix products, block_step(): jnp.einsum('hts,hsv->htv', scores, v_blk)  21.4 us
    dot_general x16, matrix products, block_step(): jnp.einsum('hsv,hsk->hvk', v_blk * weights[:, :, None], k_blk)  18.7 us
    dot_general x16, matrix products, block_step(): jnp.einsum('htd,hsd->hts', q_blk, k_blk)  17.1 us
    dot_general x16, matrix products, block_step(): jnp.einsum('hvk,htk->htv', memory, q_blk)  16.2 us
    dot_general x16, matrix products, block_step(): jnp.einsum('hs,hsk->hk', weights, k_blk)  15.6 us
    all_to_all x1, blocking collectives, per_device(): owned = lax.all_to_all(mixed, 'tp', split_axis=0, concat_axis=1, tiled=True)  15.5 us
  transfers between devices with their start and end apart: 4, of which 1 were waited for; matrix products, arithmetic and copies ran while one was open for 7% of the time, Pallas kernels for 0%

profile of v1, /device:TPU:1, one launch (start us, length us, event | category | flops | bytes accessed | tf_op | source)
XLA Modules:
  0.0 400.5 jit_solution(15390025948402802978)
XLA Ops:
  6.5 3.7 stack.37
  10.2 5.0 %all-to-all-start = ((bf16[4,1024,512]{2,1,0:T(8,128)(2,1)}), bf16[4,1024,512]{2,1,0:T(8,128)(2,1)}, u32[]{:S(2)}, u32[]{:S(2)}) async-start(bf16[4,1024,512]{2,1,0:T(8,128)(2,1)} %stack.37), calls=%async_computation | async-start | bytes 8388608 | tf_op jit(solution)/shard_map/all_to_all | solution.py:185
  16.5 2.0 constant_dynamic-update-slice_fusion.8
  19.7 2.3 constant_dynamic-update-slice_fusion.6
  24.2 39.7 %all-to-all-done = bf16[4,1024,512]{2,1,0:T(8,128)(2,1)} async-done(((bf16[4,1024,512]{2,1,0:T(8,128)(2,1)}), bf16[4,1024,512]{2,1,0:T(8,128)(2,1)}, u32[]{:S(2)}, u32[]{:S(2)}) %all-to-all-start) | async-done | bytes 4194336 | tf_op jit(solution)/shard_map/all_to_all | solution.py:185
  63.9 6.3 %copy.123 = bf16[4,1024,512]{1,2,0:T(8,128)(2,1)} copy(bf16[4,1024,512]{2,1,0:T(8,128)(2,1)} %all-to-all-done) | data formatting | bytes 8388608 | tf_op jit(solution)/shard_map/all_to_all | solution.py:185
  70.2 3.5 convert_reduce_fusion
  73.8 2.7 fusion.68
  76.5 1.3 multiply_convert_fusion
  80.2 8.9 %convolution_convert_fusion = bf16[1024,1152]{1,0:T(8,128)(2,1)S(1)} fusion(bf16[1024,2048]{0,1:T(8,128)(2,1)} %fusion.68, bf16[2048,1152]{1,0:T(8,128)(2,1)} %constant_dynamic-update-slice_fusion.4), kind=kOutput, calls=%fused_computation.123 | convolution fusion | flops 4833017856 | bytes 11272192 | tf_op jit(solution)/shard_map/dot_general | solution.py:195
  89.1 1.5 multiply_bitcast_fusion
  90.9 5.1 %rev.20 = f32[2,1024,128]{2,1,0:T(8,128)} reverse(f32[2,1024,128]{2,1,0:T(8,128)S(1)} %bitcast.510), dimensions={1} | reverse | bytes 2097152 | tf_op jit(solution)/shard_map/rev | solution.py:229
  95.9 2.5 copy_bitcast_fusion
  98.5 8.2 %rev.22 = bf16[2,1024,128]{2,1,0:T(8,128)(2,1)} reverse(bf16[2,1024,128]{2,1,0:T(8,128)(2,1)} %get-tuple-element.431), dimensions={1} | reverse | bytes 1048576 | tf_op jit(solution)/shard_map/rev | solution.py:225
  106.7 1.9 copy.250
  108.6 8.2 %rev.21 = bf16[2,1024,128]{2,1,0:T(8,128)(2,1)} reverse(bf16[2,1024,128]{2,1,0:T(8,128)(2,1)} %get-tuple-element.405), dimensions={1} | reverse | bytes 1048576 | tf_op jit(solution)/shard_map/rev | solution.py:228
  117.9 65.9 %while.43 = (s32[]{:T(128)}, f32[2,128,128]{2,1,0:T(8,128)S(1)}, f32[2,128]{1,0:T(2,128)S(1)}, f32[2]{0:T(128)S(1)}, f32[8,2,128,128]{3,2,1,0:T(8,128)}, /*index...) while((s32[]{:T(128)}, f32[2,128,128]{2,1,0:T(8,128)S(1)}, ...), condition=%wide.region_18.19_spmd.clone, body=%wide.region_13.18_spmd.clone.sunk | while | flops 34327816 | bytes 1600317 | solution.py:75
  124.4 1.8 fusion.264
  132.6 1.8 fusion.264
  140.9 1.8 fusion.264
  149.1 1.8 fusion.264
  157.3 1.8 fusion.264
  165.6 1.8 fusion.264
  173.8 1.8 fusion.264
  182.1 1.8 fusion.264
  183.9 1.9 copy.251
  186.9 58.1 %while.42 = (s32[]{:T(128)}, f32[2,128,128]{2,1,0:T(8,128)S(1)}, f32[2,128]{1,0:T(2,128)S(1)}, f32[2]{0:T(128)S(1)}, f32[8,2,128,128]{3,2,1,0:T(8,128)}, /*index...) while((s32[]{:T(128)}, f32[2,128,128]{2,1,0:T(8,128)S(1)}, ...), condition=%wide.region_7.8_spmd.clone, body=%wide.region_2.7_spmd.clone.sunk | while | flops 34327816 | bytes 1600821 | solution.py:75
  249.6 27.5 %all-gather.4 = f32[32,2,2]{2,1,0:T(2,128)S(1)} all-gather(f32[1,2,2]{2,1,0:T(2,128)S(1)} %maximum_bitcast_fusion), channel_id=2, replica_groups=mesh['sp'=32,'tp'=4] {'sp'}, dimensions={0}, use_global_device_ids=true | all-gather | bytes 528 | tf_op jit(solution)/shard_map/all_gather | solution.py:259
  278.2 2.9 collective-permute-start
  281.2 1.9 collective-permute-start.1
  283.2 26.7 %all-gather.5 = f32[32,2,2]{2,1,0:T(2,128)S(1)} all-gather(f32[1,2,2]{2,1,0:T(2,128)S(1)} %maximum_bitcast_fusion.1), channel_id=3, replica_groups=mesh['sp'=32,'tp'=4] {'sp'}, dimensions={0}, use_global_device_ids=true | all-gather | bytes 528 | tf_op jit(solution)/shard_map/all_gather | solution.py:259
  310.5 21.5 %all-gather.3 = bf16[64,2,128]{2,1,0:T(2,128)(2,1)S(1)} all-gather(bf16[2,2,128]{2,1,0:T(2,128)(2,1)S(1)} %pad_maximum_fusion.3), channel_id=5, replica_groups=mesh['sp'=32,'tp'=4] {'sp'}, dimensions={0}, use_global_device_ids=true | all-gather | bytes 33792 | tf_op jit(solution)/shard_map/all_gather | solution.py:259
  332.4 1.3 fusion.173
  335.4 2.6 copy.146
  338.0 2.4 reshape.667
  340.5 1.3 copy.152
  341.8 2.4 reshape.670
  344.2 2.1 fusion.79
  346.3 4.2 %slice_bitcast_fusion.1 = (bf16[32,2,128,128]{3,2,1,0:T(8,128)(2,1)}, bf16[32,2,128,128]{3,2,1,0:T(8,128)(2,1)S(1)}) fusion(bf16[32,2,2,128,128]{4,3,2,1,0:T(8,128)(2,1)} %bitcast.514), kind=kLoop, calls=%fused_computation.118 | loop fusion | bytes 8388608 | tf_op jit(solution)/shard_map/squeeze | solution.py:260
  351.8 1.3 fusion.78
  353.2 9.4 %rev.23 = f32[2,1024,128]{1,2,0:T(8,128)} reverse(f32[2,1024,128]{1,2,0:T(8,128)} %fusion.78), dimensions={1} | reverse | bytes 2097152 | tf_op jit(solution)/shard_map/rev | solution.py:273
  362.6 2.8 fusion.71
  365.4 2.0 fusion.171
  368.7 1.6 copy.190
  370.3 1.3 multiply_convert_fusion.1
  372.9 15.5 %all_to_all.21 = bf16[4,256,384]{1,2,0:T(8,128)(2,1)S(1)} all-to-all(bf16[4,256,384]{1,2,0:T(8,128)(2,1)} %copy.155), channel_id=1, replica_groups=mesh['sp'=32,'tp'=4] {'tp'}, dimensions={0} | all-to-all | bytes 1572864 | tf_op jit(solution)/shard_map/all_to_all | solution.py:285
  388.5 3.5 fusion.174
  391.9 1.7 fusion.73
  (414 shorter events, 130.9 us)
Async XLA Ops:
  6.5 385.4 %copy-start = (bf16[512,2048]{1,0:T(8,128)(2,1)S(1)}, bf16[512,2048]{1,0:T(8,128)(2,1)}, u32[]{:S(2)}) copy-start(bf16[512,2048]{1,0:T(8,128)(2,1)} %param.42) | copy-start | bytes 6291460
  10.2 5.1 %copy-start.10 = (f32[2048]{0:T(1024)S(1)}, f32[2048]{0:T(1024)}, u32[]{:S(2)}) copy-start(f32[2048]{0:T(1024)} %param.25) | copy-start | bytes 24580
  10.2 6.2 %copy-start.14 = (f32[2,8]{1,0:T(2,128)S(1)}, f32[2,8]{1,0:T(2,128)}, u32[]{:S(2)}) copy-start(f32[2,8]{1,0:T(2,128)} %param.33) | copy-start | bytes 196
  10.2 8.3 %copy-start.6 = (bf16[2048,256]{1,0:T(8,128)(2,1)S(1)}, bf16[2048,256]{1,0:T(8,128)(2,1)}, u32[]{:S(2)}) copy-start(bf16[2048,256]{1,0:T(8,128)(2,1)} %param.27) | copy-start | bytes 3145732
  10.2 53.7 %all-to-all-start = ((bf16[4,1024,512]{2,1,0:T(8,128)(2,1)}), bf16[4,1024,512]{2,1,0:T(8,128)(2,1)}, u32[]{:S(2)}, u32[]{:S(2)}) async-start(bf16[4,1024,512]{2,1,0:T(8,128)(2,1)} %stack.37), calls=%async_computation | async-start | bytes 8388608 | tf_op jit(solution)/shard_map/all_to_all | solution.py:185
  15.3 331.0 %all-gather.8.cloned.1.call-start = ((), (), s32[]{:S(2)}) async-start(), calls=%async_computation.2 | async-start | bytes 4325376 | tf_op jit(solution)/shard_map/all_gather | solution.py:259
  16.4 5.5 %copy-start.7 = (bf16[2048,256]{1,0:T(8,128)(2,1)S(1)}, bf16[2048,256]{1,0:T(8,128)(2,1)}, u32[]{:S(2)}) copy-start(bf16[2048,256]{1,0:T(8,128)(2,1)} %param.29) | copy-start | bytes 3145732
  16.5 6.6 %copy-start.8 = (bf16[2048,256]{1,0:T(8,128)(2,1)S(1)}, bf16[2048,256]{1,0:T(8,128)(2,1)}, u32[]{:S(2)}) copy-start(bf16[2048,256]{1,0:T(8,128)(2,1)} %param.30) | copy-start | bytes 3145732
  70.2 3.5 copy-start.1
  77.8 1.6 copy-start.11
  77.8 1.6 copy-start.12
  89.1 1.8 copy-start.5
  186.9 123.3 %copy-start.15 = (f32[2,2]{1,0:T(2,128)S(1)}, f32[2,2]{1,0:T(2,128)}, u32[]{:S(2)}) copy-start(f32[2,2]{1,0:T(2,128)} %param.38) | copy-start | bytes 52
  186.9 145.5 %copy-start.13 = (f32[2,2,128]{2,1,0:T(2,128)S(1)}, f32[2,2,128]{2,1,0:T(2,128)}, u32[]{:S(2)}) copy-start(f32[2,2,128]{2,1,0:T(2,128)} %param.37) | copy-start | bytes 6148
  244.9 95.6 %copy-start.4 = (f32[8,2,128,128]{3,2,1,0:T(8,128)S(1)}, f32[8,2,128,128]{3,2,1,0:T(8,128)}, u32[]{:S(2)}) copy-start(f32[8,2,128,128]{3,2,1,0:T(8,128)} %get-tuple-element.149) | copy-start | bytes 3145732
  278.2 65.9 %collective-permute-start = (bf16[8,128]{1,0:T(8,128)(2,1)S(1)}, bf16[8,128]{1,0:T(8,128)(2,1)S(1)}, u32[]{:S(2)}, u32[]{:S(2)}) collective-permute-start(bf16[8,128]{1,0:T(8,128)(2,1)S(1)} %get-tuple-element.397), channel_id=1, source_target_pairs={{0,4},{4,8},{8,12},{12,16},{16,20},{20,24},{24,28},{28,32},{32,36}... | collective-permute-start | bytes 6152 | tf_op jit(solution)/shard_map/ppermute | solution.py:19
  281.2 63.0 %collective-permute-start.1 = (bf16[8,128]{1,0:T(8,128)(2,1)S(1)}, bf16[8,128]{1,0:T(8,128)(2,1)S(1)}, u32[]{:S(2)}, u32[]{:S(2)}) collective-permute-start(bf16[8,128]{1,0:T(8,128)(2,1)S(1)} %get-tuple-element.398), channel_id=1, source_target_pairs={{4,0},{8,4},{12,8},{16,12},{20,16},{24,20},{28,24},{32,28},{36,32}... | collective-permute-start | bytes 6152 | tf_op jit(solution)/shard_map/ppermute | solution.py:22
  335.4 8.7 %slice-start = ((bf16[1024,1152]{1,0:T(8,128)(2,1)}), bf16[1024,128]{1,0:T(8,128)(2,1)S(1)}, s32[]{:S(2)}) async-start(bf16[1024,1152]{1,0:T(8,128)(2,1)} %copy-done.5), calls=%async_computation.3 | async-start | bytes 524288 | tf_op jit(solution)/shard_map/slice | solution.py:197
  346.3 5.5 %copy-start.3 = (bf16[2,1024,128]{2,1,0:T(8,128)(2,1)S(1)}, bf16[2,1024,128]{2,1,0:T(8,128)(2,1)}, u32[]{:S(2)}) copy-start(bf16[2,1024,128]{2,1,0:T(8,128)(2,1)} %rev.22) | copy-start | bytes 1572868
  346.3 5.5 %copy-start.9 = (f32[2,1024,128]{1,2,0:T(8,128)S(1)}, f32[2,1024,128]{1,2,0:T(8,128)}, u32[]{:S(2)}) copy-start(f32[2,1024,128]{1,2,0:T(8,128)} %reshape.670) | copy-start | bytes 3145732
  346.3 5.5 %copy-start.16 = (f32[2,2,128,128]{3,2,1,0:T(8,128)S(1)}, f32[2,2,128,128]{3,2,1,0:T(8,128)}, u32[]{:S(2)}) copy-start(f32[2,2,128,128]{3,2,1,0:T(8,128)} %param.36) | copy-start | bytes 786436
  351.8 13.6 %copy-start.2 = (bf16[128,2,8,128]{3,2,1,0:T(8,128)(2,1)S(1)}, bf16[128,2,8,128]{3,2,1,0:T(8,128)(2,1)}, u32[]{:S(2)}) copy-start(bf16[128,2,8,128]{3,2,1,0:T(8,128)(2,1)} %get-tuple-element.400) | copy-start | bytes 1572868
Sparse Core Ops, SparseCore 0:
  245.7 48.4 all-gather.7
